TPU v7x, 32 devices: a whole 2x2x4 slice. The times are simulated.
32 devices in a mesh: ep: 8 (over z, x), tp: 4 (over y, core).
Axes of the slice: x: 2, y: 2, z: 4, core: 2. Of those that a mesh axis runs over, the one named last changes fastest.
Arguments:
- tokens: bfloat16 [8192, 2048], P(('ep', 'tp')), may hold values from -6 to 6
- pre_gain: float32 [2048], replicated, may hold values from 0.1 to 1.9
- post_gain: float32 [2048], replicated, may hold values from 0.1 to 1.9
- expert_ids: int32 [8192, 2], P(('ep', 'tp')), may hold values from 0 to 7, as said below
- route_weight: float32 [8192, 2], P(('ep', 'tp')), may hold values from 0.1 to 1
- w_gate: bfloat16 [8, 2048, 512], P('ep', None, 'tp'), may hold values from -0.125 to 0.125
- w_up: bfloat16 [8, 2048, 512], P('ep', None, 'tp'), may hold values from -0.125 to 0.125
- w_down: bfloat16 [8, 2048, 512], P('ep', None, 'tp'), may hold values from -0.25 to 0.25
Outputs:
- layer_out: bfloat16 [8192, 2048], P(('ep', 'tp'))
Inputs may be any that keep to these rules, and one draw needn't show every extreme that they name: `expert_ids`: each token names two different experts of one group, group g being experts 4 * g to 4 * g + 3. Among the rows of one device (aligned blocks of 256 rows) no expert is named more than 128 times, and in every block some expert is named exactly 128 times; one expert is named 128 times in every block.
All inputs are finite; a program needn't handle non-finite values.
Results may differ from a plain program's by a relative error of at most 0.0071.
Values may be sent and summed in bfloat16 or wider, within the bound.
A program may use at most 64 MiB of HBM per device.

v0:
```python
import functools

import jax
import jax.numpy as jnp
from jax import lax
from jax.experimental import pallas as pl
from jax.experimental.pallas import tpu as pltpu
from jax.sharding import PartitionSpec as P


def rms_scale(values, gain):
    mean_sq = jnp.mean(values * values, axis=-1, keepdims=True)
    return values * lax.rsqrt(mean_sq + 1e-06) * gain


def expert_terms(rows, gate_part, up_part, down_part):
    gate = jnp.dot(rows, gate_part, preferred_element_type=jnp.float32)
    up = jnp.dot(rows, up_part, preferred_element_type=jnp.float32)
    hidden = (jax.nn.silu(gate) * up).astype(jnp.bfloat16)
    return lax.dot_general(
        hidden, down_part, (((1,), (1,)), ((), ())), preferred_element_type=jnp.float32
    )


def collect_expert(w_gate, w_up, w_down):
    return (
        lax.all_gather(w_gate, "tp", axis=2, tiled=True),
        lax.all_gather(w_up, "tp", axis=2, tiled=True),
        lax.all_gather(w_down, "tp", axis=2, tiled=True),
    )


def body(tokens, pre_gain, post_gain, expert_ids, route_weight, w_gate, w_up, w_down):
    count, width = tokens.shape
    top = expert_ids.shape[1]
    experts = lax.axis_size("ep") * w_gate.shape[0]
    capacity = 2 * top * count // experts
    normed = rms_scale(tokens.astype(jnp.float32), pre_gain).astype(jnp.bfloat16)
    flat = expert_ids.reshape(-1)
    onehot = (flat[:, None] == jnp.arange(experts, dtype=jnp.int32)[None, :]).astype(jnp.int32)
    rank = jnp.sum((jnp.cumsum(onehot, axis=0) - onehot) * onehot, axis=1)
    target = flat * capacity + rank
    source = jnp.full((experts * capacity,), count, jnp.int32)
    source = source.at[target].set(jnp.arange(count * top, dtype=jnp.int32) // top)
    padded = jnp.concatenate([normed, jnp.zeros((1, width), jnp.bfloat16)], axis=0)
    outgoing = padded[source].reshape(experts, capacity, width)
    arrived = lax.all_to_all(outgoing, "ep", split_axis=0, concat_axis=0, tiled=True)
    rows = arrived.reshape(experts * capacity, width)
    gate_all, up_all, down_all = collect_expert(w_gate, w_up, w_down)
    result = expert_terms(rows, gate_all[0], up_all[0], down_all[0])
    answer = result.astype(jnp.bfloat16).reshape(experts, capacity, width)
    returned = lax.all_to_all(answer, "ep", split_axis=0, concat_axis=0, tiled=True)
    per_route = returned.reshape(experts * capacity, width)[target].reshape(count, top, width)
    mixed = jnp.sum(per_route.astype(jnp.float32) * route_weight[:, :, None], axis=1)
    return rms_scale(mixed, post_gain).astype(jnp.bfloat16)

MESH = pl.DeviceIdType.MESH
GU_CUTS = 8
DOWN_CUTS = 8
LAG = 5
TOKEN_CUTS = 8
VMEM_BYTES = 60 * 2**20


def flip(index, stride):
    return index + stride - 2 * stride * lax.rem(lax.div(index, stride), 2)


def kernel(
    n_ep, tok, pre, post, wr, wg, wu, wd, out,
    T, X, WR, COL, GU, DN, H, S, R, PZ, ZS, ZR, ACC,
    loc, t_send, t_recv, w_send, w_recv, g_send, g_recv, d_send, d_recv, x_send, x_recv, z_send, z_recv,
):
    count, width = tok.shape
    part = wg.shape[2]
    experts = wr.shape[0]
    half = n_ep // 2
    e, t = lax.axis_index("ep"), lax.axis_index("tp")
    to_x, to_z, to_h = (flip(e, 1), t), (flip(e, 2), t), (flip(e, half), t)
    to_c, to_y = (e, flip(t, 1)), (e, flip(t, 2))

    barrier = pltpu.get_barrier_semaphore()
    for who in (to_x, to_z, to_h, to_c, to_y):
        pl.semaphore_signal(barrier, inc=1, device_id=who, device_id_type=MESH)

    own = [
        pltpu.make_async_copy(tok, T.at[0], loc.at[0]),
        pltpu.make_async_copy(wr, WR.at[0], loc.at[1]),
        pltpu.make_async_copy(wg.at[0], GU.at[0, :, pl.ds(0, part)], loc.at[2]),
        pltpu.make_async_copy(wu.at[0], GU.at[0, :, pl.ds(part, part)], loc.at[3]),
        pltpu.make_async_copy(wd.at[0], DN.at[:, pl.ds(0, part)], loc.at[4]),
    ]
    for copy in own:
        copy.start()

    def remote(src, dst, send, recv, who):
        return pltpu.make_async_remote_copy(
            src_ref=src, dst_ref=dst, send_sem=send, recv_sem=recv, device_id=who, device_id_type=MESH
        )

    block_from = {1: (0, to_z), 2: (0, to_x), 3: (1, to_x)}
    sent = []

    def routes_copy(k):
        s, who = block_from[k]
        return (remote(WR.at[s], WR.at[k], w_send.at[k], w_recv.at[k], who),)

    t_rows = count // TOKEN_CUTS

    def tokens_copy(k, j):
        s, who = block_from[k]
        rows = pl.ds(j * t_rows, t_rows)
        return (remote(T.at[s, rows], T.at[k, rows], t_send.at[k, j], t_recv.at[k, j], who),)

    def route(k):
        if k % 2:
            return k - 1, to_c
        if k % 4:
            return k - 2, to_y
        return 0, to_h

    g_rows, d_rows = width // GU_CUTS, width // DOWN_CUTS

    def gu_copy(k, j):
        s, who = route(k)
        rows = pl.ds(j * g_rows, g_rows)
        return (remote(GU.at[s, rows], GU.at[k, rows], g_send.at[k, j], g_recv.at[k, j], who),)

    def dn_copy(k, j):
        s, who = route(k)
        rows = pl.ds(j * d_rows, d_rows)
        return (
            remote(
                DN.at[rows, pl.ds(s * part, part)], DN.at[rows, pl.ds(k * part, part)],
                d_send.at[k, j], d_recv.at[k, j], who,
            ),
        )

    def go(copies):
        for copy in copies:
            copy.start()
            sent.append(copy)

    def arrive(copies):
        for copy in copies:
            copy.wait_recv()

    def norm(block):
        rows = pl.ds(block * count, count)

        def some(i, carry):
            part_rows = pl.ds(pl.multiple_of(i * 32, 32), 32)
            values = T[block, part_rows, :].astype(jnp.float32)
            X[pl.ds(pl.multiple_of(block * count + i * 32, 32), 32), :] = rms_scale(values, pre[...]).astype(jnp.bfloat16)
            return carry

        lax.fori_loop(0, count // 32, some, 0)
        eye = lax.broadcasted_iota(jnp.int32, (count, count), 0) == lax.broadcasted_iota(
            jnp.int32, (count, count), 1
        )
        which = lax.broadcasted_iota(jnp.int32, (experts, count), 0)
        table = WR[block]
        for h in range(2):
            expert = lax.rem(e + h * half, n_ep)
            row = jnp.sum(jnp.where(which == expert, table, 0.0), axis=0, keepdims=True)
            col = jnp.sum(jnp.where(eye, row, 0.0), axis=1, keepdims=True)
            COL[h, rows, :] = jnp.broadcast_to(col, (count, part))

    def hidden(slots, blocks):
        low, high = slots
        first, last = blocks
        rows = pl.ds(first * count, (last - first) * count)

        def one(s, carry):
            left = X[rows, :]
            both = jnp.dot(left, GU[s], preferred_element_type=jnp.float32)
            gate, up = both[:, :part], both[:, part:]
            value = gate / (1.0 + jnp.exp(-gate)) * up * COL[lax.div(s, 4), rows, :]
            H[rows, pl.ds(pl.multiple_of(s * part, part), part)] = value.astype(jnp.bfloat16)
            return carry

        lax.fori_loop(low, high, one, 0)

    for copy in own[:2]:
        copy.wait()
    pl.semaphore_wait(barrier, 5)
    for k in (1, 2):
        go(routes_copy(k))
    for copy in own[2:4]:
        copy.wait()
    for j in range(TOKEN_CUTS):
        go(tokens_copy(1, j))
        go(tokens_copy(2, j))
        for i in range(j * GU_CUTS // TOKEN_CUTS, (j + 1) * GU_CUTS // TOKEN_CUTS):
            for k in (4, 2, 1):
                go(gu_copy(k, i))
    own[4].wait()
    for j in range(DOWN_CUTS):
        go(dn_copy(1, j))
    norm(0)
    for j in range(GU_CUTS):
        arrive(gu_copy(1, j))
    hidden((0, 2), (0, 1))
    arrive(routes_copy(1))
    go(routes_copy(3))
    arrive(routes_copy(2))

    def tokens_on(low, high):
        for i in range(low, high):
            arrive(tokens_copy(1, i))
            go(tokens_copy(3, i))

    half_t, half_g = TOKEN_CUTS // 2, GU_CUTS // 2
    tokens_on(0, half_t)
    for j in range(GU_CUTS):
        arrive(gu_copy(2, j))
        go(gu_copy(3, j))
    for j in range(TOKEN_CUTS):
        arrive(tokens_copy(2, j))

    def fourth(low, high):
        for j in range(low, high):
            arrive(gu_copy(4, j))
            go(gu_copy(6, j))
            go(gu_copy(5, j))
            span = TOKEN_CUTS - half_t
            tokens_on(half_t + span * j // GU_CUTS, half_t + span * (j + 1) // GU_CUTS)

    fourth(0, half_g)
    norm(2)
    fourth(half_g, half_g + 1)
    hidden((0, 2), (2, 3))
    for j in range(GU_CUTS):
        arrive(gu_copy(3, j))
    fourth(half_g + 1, half_g + 2)
    hidden((2, 4), (0, 1))
    fourth(half_g + 2, half_g + 3)
    hidden((2, 4), (2, 3))
    fourth(half_g + 3, GU_CUTS)
    for j in range(DOWN_CUTS):
        go(dn_copy(4, j))
    go(dn_copy(2, 0))
    go(dn_copy(2, 1))
    norm(1)
    for j in range(GU_CUTS):
        arrive(gu_copy(5, j))
    for j in range(GU_CUTS // 2):
        arrive(gu_copy(6, j))
        go(gu_copy(7, j))
    hidden((0, 6), (1, 2))
    for j in range(GU_CUTS // 2, GU_CUTS):
        arrive(gu_copy(6, j))
        go(gu_copy(7, j))
    hidden((4, 6), (0, 1))
    hidden((4, 6), (2, 3))
    down_next = lambda j: (arrive(dn_copy(4, j)), go(dn_copy(6, j)), go(dn_copy(5, j)))
    arrive(routes_copy(3))
    for j in range(TOKEN_CUTS):
        arrive(tokens_copy(3, j))
    norm(3)
    down_next(0)
    go(dn_copy(2, 2))
    hidden((0, 7), (3, 4))
    hidden((6, 7), (0, 3))
    arrive(dn_copy(2, 0))
    go(dn_copy(3, 0))
    down_next(1)
    go(dn_copy(2, 3))
    arrive(dn_copy(6, 0))
    go(dn_copy(7, 0))
    for j in range(GU_CUTS):
        arrive(gu_copy(7, j))
    hidden((7, 8), (0, 4))

    def down(block, j):
        return lax.dot_general(
            H[pl.ds(block * count, count), :], DN[pl.ds(j * d_rows, d_rows), :],
            (((1,), (1,)), ((), ())), preferred_element_type=jnp.float32,
        )

    def first_copy(j):
        return (remote(S.at[j], R.at[j], x_send.at[j], x_recv.at[j], to_z if j % 2 else to_x),)

    def second_copy(j):
        return (remote(ZS.at[j], ZR.at[j], z_send.at[j], z_recv.at[j], to_x if j % 2 else to_z),)

    def pass_on(j):
        arrive(first_copy(j))
        ZS[j] = (PZ[j] + R[j, count:].astype(jnp.float32)).astype(jnp.bfloat16)
        go(second_copy(j))
        ACC[j] = ACC[j] + R[j, :count].astype(jnp.float32)

    for j in range(DOWN_CUTS):
        if j + 2 < DOWN_CUTS:
            down_next(j + 2)
        if j + 4 < DOWN_CUTS:
            go(dn_copy(2, j + 4))
        if j + 1 < DOWN_CUTS:
            arrive(dn_copy(2, j + 1))
            go(dn_copy(3, j + 1))
            arrive(dn_copy(6, j + 1))
            go(dn_copy(7, j + 1))
        for k in (1, 3, 5, 7):
            arrive(dn_copy(k, j))
        near, kept = (1, 2) if j % 2 else (2, 1)
        S[j, count:] = down(3, j).astype(jnp.bfloat16)
        S[j, :count] = down(near, j).astype(jnp.bfloat16)
        go(first_copy(j))
        PZ[j] = down(kept, j)
        ACC[j] = down(0, j)
        if j >= LAG:
            pass_on(j - LAG)
    for j in range(DOWN_CUTS - LAG, DOWN_CUTS):
        pass_on(j)
    square = jnp.zeros((count, 1), jnp.float32)
    for j in range(DOWN_CUTS):
        arrive(second_copy(j))
        mixed = ACC[j] + ZR[j].astype(jnp.float32)
        ACC[j] = mixed
        square = square + jnp.sum(mixed * mixed, axis=1, keepdims=True)
    scale = lax.rsqrt(square / width + 1e-06)
    for j in range(DOWN_CUTS):
        cols = pl.ds(j * d_rows, d_rows)
        out[:, cols] = (ACC[j] * scale * post[:, cols]).astype(jnp.bfloat16)
    for copy in sent:
        copy.wait_send()


def fused(n_ep, tokens, pre_gain, post_gain, expert_ids, route_weight, w_gate, w_up, w_down):
    count, width = tokens.shape
    part = w_gate.shape[2]
    experts = n_ep * w_gate.shape[0]
    names = jnp.arange(experts, dtype=jnp.int32)[:, None, None]
    picks = jnp.where(expert_ids.T[None] == names, route_weight.T[None], 0.0)
    wr = jnp.sum(picks, axis=1)
    bf, f32 = jnp.bfloat16, jnp.float32
    cols = width // DOWN_CUTS
    anywhere = pl.BlockSpec(memory_space=pl.ANY)
    vmem = pl.BlockSpec(memory_space=pltpu.VMEM)
    dma = pltpu.SemaphoreType.DMA
    return pl.pallas_call(
        functools.partial(kernel, n_ep),
        out_shape=jax.ShapeDtypeStruct((count, width), bf),
        in_specs=[anywhere, vmem, vmem, anywhere, anywhere, anywhere, anywhere],
        out_specs=vmem,
        scratch_shapes=[
            pltpu.VMEM((4, count, width), bf),
            pltpu.VMEM((4 * count, width), bf),
            pltpu.VMEM((4, experts, count), f32),
            pltpu.VMEM((2, 4 * count, part), f32),
            pltpu.VMEM((8, width, 2 * part), bf),
            pltpu.VMEM((width, 8 * part), bf),
            pltpu.VMEM((4 * count, 8 * part), bf),
            pltpu.VMEM((DOWN_CUTS, 2 * count, cols), bf),
            pltpu.VMEM((DOWN_CUTS, 2 * count, cols), bf),
            pltpu.VMEM((DOWN_CUTS, count, cols), f32),
            pltpu.VMEM((DOWN_CUTS, count, cols), bf),
            pltpu.VMEM((DOWN_CUTS, count, cols), bf),
            pltpu.VMEM((DOWN_CUTS, count, cols), f32),
            dma((5,)),
            dma((4, TOKEN_CUTS)), dma((4, TOKEN_CUTS)), dma((4,)), dma((4,)),
            dma((8, GU_CUTS)), dma((8, GU_CUTS)), dma((8, DOWN_CUTS)), dma((8, DOWN_CUTS)),
            dma((DOWN_CUTS,)), dma((DOWN_CUTS,)), dma((DOWN_CUTS,)), dma((DOWN_CUTS,)),
        ],
        compiler_params=pltpu.CompilerParams(
            collective_id=0, has_side_effects=True, vmem_limit_bytes=VMEM_BYTES
        ),
    )(tokens, pre_gain[None], post_gain[None], wr, w_gate, w_up, w_down)


def whole_body(n_ep, n_tp, *args):
    lanes = args[5].shape[2]
    if n_ep // 2 == n_tp == 2 * 2 and args[5].shape[0] == 1 and lanes % 128 == 0:
        return fused(n_ep, *args)
    return body(*args)


def solution(mesh):
    in_specs = (
        P(("ep", "tp"), None),
        P(),
        P(),
        P(("ep", "tp"), None),
        P(("ep", "tp"), None),
        P("ep", None, "tp"),
        P("ep", None, "tp"),
        P("ep", None, "tp"),
    )
    out_specs = P(("ep", "tp"), None)
    step = functools.partial(whole_body, mesh.shape["ep"], mesh.shape["tp"])
    return jax.shard_map(step, mesh=mesh, in_specs=in_specs, out_specs=out_specs, check_vma=False)
```

profile of v0, /device:TPU:0, one launch (start us, length us, event | category | flops | bytes accessed | tf_op | source)
XLA Modules:
  0.0 119.4 jit_solution(5759111582034399667)
XLA Ops:
  0.0 0.0 copy-start.1
  0.0 0.0 copy-start
  0.0 0.7 copy-done.1
  0.7 0.0 copy-done
  0.7 0.6 select_reduce_fusion.wr
  1.3 115.8 %shard_map.82 = bf16[256,2048]{1,0:T(8,128)(2,1)} custom-call(bf16[256,2048]{1,0:T(8,128)(2,1)} %tok.1, f32[1,2048]{1,0:T(1,128)} %bitcast.4, f32[1,2048]{1,0:T(1,128)} %bitcast.5, f32[8,256]{1,0:T(8,128)} %select_reduce_fusion.wr, bf16[1,2048,128]{2,1,0:T(8,128)(2,1)} %wg.1, bf16[1,2048,128]{2,1,0:T(8,128)(2,1)} %wu.1, bf16[1,2048,128]{2,1,0:T(8,128)(2,1)} %wd.1), custom_call_target="tpu_custom_call" | custom-call | tf_op jit(solution)/shard_map/pallas_call | solution.py:341
  117.1 2.3 %copy.10 = bf16[256,2048]{1,0:T(8,128)(2,1)} copy(bf16[256,2048]{1,0:T(8,128)(2,1)} %shard_map.82) | data formatting | bytes 2097152
Async XLA Ops:
  0.0 0.7 copy-start.1
  0.0 0.7 copy-start
where the time goes:
time: 121 us; the launch traced here: 119 us
  Pallas kernels  116 us (96%)
  local copies, waits for them, and re-layouts  3 us (2%)
    pallas_call x1, Pallas kernels, fused(): pl.pallas_call(functools.partial(kernel, n_ep), out_shape=jax.ShapeDtypeS...  116 us
    unnamed x5, local copies, waits for them, and re-layouts  3 us

commit v1 on v0

v1 whole, which is shorter than its diff:
```python
import functools

import jax
import jax.numpy as jnp
from jax import lax
from jax.experimental import pallas as pl
from jax.experimental.pallas import tpu as pltpu
from jax.sharding import PartitionSpec as P


def rms_scale(values, gain):
    mean_sq = jnp.mean(values * values, axis=-1, keepdims=True)
    return values * lax.rsqrt(mean_sq + 1e-06) * gain


def expert_terms(rows, gate_part, up_part, down_part):
    gate = jnp.dot(rows, gate_part, preferred_element_type=jnp.float32)
    up = jnp.dot(rows, up_part, preferred_element_type=jnp.float32)
    hidden = (jax.nn.silu(gate) * up).astype(jnp.bfloat16)
    return lax.dot_general(
        hidden, down_part, (((1,), (1,)), ((), ())), preferred_element_type=jnp.float32
    )


def collect_expert(w_gate, w_up, w_down):
    return (
        lax.all_gather(w_gate, "tp", axis=2, tiled=True),
        lax.all_gather(w_up, "tp", axis=2, tiled=True),
        lax.all_gather(w_down, "tp", axis=2, tiled=True),
    )


def body(tokens, pre_gain, post_gain, expert_ids, route_weight, w_gate, w_up, w_down):
    count, width = tokens.shape
    top = expert_ids.shape[1]
    experts = lax.axis_size("ep") * w_gate.shape[0]
    capacity = 2 * top * count // experts
    normed = rms_scale(tokens.astype(jnp.float32), pre_gain).astype(jnp.bfloat16)
    flat = expert_ids.reshape(-1)
    onehot = (flat[:, None] == jnp.arange(experts, dtype=jnp.int32)[None, :]).astype(jnp.int32)
    rank = jnp.sum((jnp.cumsum(onehot, axis=0) - onehot) * onehot, axis=1)
    target = flat * capacity + rank
    source = jnp.full((experts * capacity,), count, jnp.int32)
    source = source.at[target].set(jnp.arange(count * top, dtype=jnp.int32) // top)
    padded = jnp.concatenate([normed, jnp.zeros((1, width), jnp.bfloat16)], axis=0)
    outgoing = padded[source].reshape(experts, capacity, width)
    arrived = lax.all_to_all(outgoing, "ep", split_axis=0, concat_axis=0, tiled=True)
    rows = arrived.reshape(experts * capacity, width)
    gate_all, up_all, down_all = collect_expert(w_gate, w_up, w_down)
    result = expert_terms(rows, gate_all[0], up_all[0], down_all[0])
    answer = result.astype(jnp.bfloat16).reshape(experts, capacity, width)
    returned = lax.all_to_all(answer, "ep", split_axis=0, concat_axis=0, tiled=True)
    per_route = returned.reshape(experts * capacity, width)[target].reshape(count, top, width)
    mixed = jnp.sum(per_route.astype(jnp.float32) * route_weight[:, :, None], axis=1)
    return rms_scale(mixed, post_gain).astype(jnp.bfloat16)

MESH = pl.DeviceIdType.MESH
CUTS = 8
NEAR_CUTS = 4
LAG = 3
AHEAD = 4
Z_FIRST = (0, 4)
PLACE = (0, 3, 1, 2)
VMEM_BYTES = 60 * 2**20


def flip(index, stride):
    return index + stride - 2 * stride * lax.rem(lax.div(index, stride), 2)


def kernel(
    n_ep, tok, pre, post, ids, rw, wg, wu, wd, out,
    T, XT, XC, IDS, RW, PRE, POST, WR, RK, COL, GU, DN, H, HX, EC, SN, SF, RN, RF, ZS, ZR, ACC,
    loc, t_send, t1_recv, t_recv, w_send, w_recv, g_send, g_recv, g2_recv, gf_recv, d_send, d_recv, df_recv,
    s_send, n_recv, m_recv, f_recv, z_recv,
):
    count, width = tok.shape
    part = wg.shape[2]
    experts = WR.shape[1]
    cap = EC.shape[2]
    half = n_ep // 2
    bf, f32 = jnp.bfloat16, jnp.float32
    e, t = lax.axis_index("ep"), lax.axis_index("tp")
    to_x, to_z, to_h = (flip(e, 1), t), (flip(e, 2), t), (flip(e, half), t)
    to_c, to_y = (e, flip(t, 1)), (e, flip(t, 2))

    barrier = pltpu.get_barrier_semaphore()
    for who in (to_x, to_z, to_h, to_c, to_y):
        pl.semaphore_signal(barrier, inc=1, device_id=who, device_id_type=MESH)

    own = [
        pltpu.make_async_copy(ids, IDS, loc.at[0]),
        pltpu.make_async_copy(rw, RW, loc.at[1]),
        pltpu.make_async_copy(tok, T.at[0], loc.at[2]),
        pltpu.make_async_copy(wg.at[0], GU.at[0, :, pl.ds(0, part)], loc.at[3]),
        pltpu.make_async_copy(wu.at[0], GU.at[0, :, pl.ds(part, part)], loc.at[4]),
        pltpu.make_async_copy(wd.at[0], DN.at[:, pl.ds(0, part)], loc.at[5]),
        pltpu.make_async_copy(pre, PRE, loc.at[6]),
        pltpu.make_async_copy(post, POST, loc.at[7]),
    ]
    for copy in own:
        copy.start()

    def remote(src, dst, send, recv, who):
        return pltpu.make_async_remote_copy(
            src_ref=src, dst_ref=dst, send_sem=send, recv_sem=recv, device_id=who, device_id_type=MESH
        )

    def rows_of(total, cuts, j):
        return pl.ds(0, total) if j is None else pl.ds(j * (total // cuts), total // cuts)

    block_from = {1: (0, to_z), 2: (0, to_x), 3: (1, to_x)}

    def routes(k):
        s, who = block_from[k]
        return remote(WR.at[s], WR.at[k], w_send.at[k - 1], w_recv.at[k - 1], who)

    def tokens(k, j=None):
        s, who = block_from[k]
        rows = rows_of(count, CUTS, j)
        recv = t1_recv.at[j] if k == 1 and j is not None else t_recv.at[k - 1]
        return remote(T.at[s, rows], T.at[k, rows], t_send.at[k - 1], recv, who)

    def route(k):
        if k % 2:
            return k - 1, to_c
        if k % 4:
            return k - 2, to_y
        return 0, to_h

    def gu(k, j=None):
        s, who = route(k)
        rows = rows_of(width, NEAR_CUTS if k in (2, 3) else CUTS, j)
        recv = g_recv.at[k - 1]
        if j is not None and k == 2:
            recv = g2_recv.at[j]
        if j is not None and k in (4, 6):
            recv = gf_recv.at[k // 2 - 2, j]
        return remote(GU.at[s, rows], GU.at[k, rows], g_send.at[k - 1], recv, who)

    def dn(k, j=None):
        s, who = route(k)
        rows = rows_of(width, CUTS, j)
        recv = d_recv.at[k - 1] if k < 4 else df_recv.at[k - 4, 0 if j is None else j]
        return remote(
            DN.at[rows, pl.ds(s * part, part)], DN.at[rows, pl.ds(k * part, part)], d_send.at[k - 1], recv, who
        )

    cols = width // CUTS

    def lane_block(j):
        return pl.ds(j * cols, cols)

    def first(kind, j, rows=None):
        src, dst = (SN, RN) if kind < 2 else (SF, RF)
        rows = pl.ds(0, 2 * cap) if rows is None else rows
        recv = (n_recv, m_recv, f_recv)[kind].at[j]
        return remote(src.at[j, rows], dst.at[j, rows], s_send.at[kind // 2], recv, to_z if j in Z_FIRST else to_x)

    def second(j):
        return remote(ZS.at[j], ZR.at[j], s_send.at[2], z_recv.at[j], to_x if j in Z_FIRST else to_z)

    which = lax.broadcasted_iota(jnp.int32, (experts, count), 0)
    mine = (e, lax.rem(e + half, n_ep))
    of_x = (flip(e, 1), lax.rem(flip(e, 1) + half, n_ep))
    of_z = (flip(e, 2), lax.rem(flip(e, 2) + half, n_ep))

    def row_of(table, expert):
        return jnp.sum(jnp.where(which == expert, table, 0.0), axis=0, keepdims=True)

    def own_routes():
        picks = [jnp.where(IDS[k : k + 1, :] == which, RW[k : k + 1, :], 0.0) for k in range(ids.shape[0])]
        total = picks[0]
        for pick in picks[1:]:
            total = total + pick
        WR[0] = total

    def ranks(block):
        named = WR[block] > 0.0
        ones = jnp.where(named, 1.0, 0.0)
        before = lax.broadcasted_iota(jnp.int32, (count, count), 0) <= lax.broadcasted_iota(
            jnp.int32, (count, count), 1
        )
        upto = jnp.dot(ones, jnp.where(before, 1.0, 0.0), preferred_element_type=f32)
        RK[block] = jnp.where(named, upto - 1.0, -1.0)

    def norm(block, slot, low, high):
        def some(i, carry):
            rows = pl.ds(pl.multiple_of(i * 16, 16), 16)
            values = T[block, rows, :].astype(f32)
            XT[slot, rows, :] = rms_scale(values, PRE[...]).astype(bf)
            return carry

        lax.fori_loop(low // 16, high // 16, some, 0)

    def gather(block, slot):
        rows = pl.ds(PLACE[block] * cap, cap)
        for h in range(2):
            at = row_of(RK[block], mine[h])
            hit = lax.broadcasted_iota(jnp.int32, (cap, count), 0).astype(f32) == at
            weight = jnp.sum(jnp.where(hit, row_of(WR[block], mine[h]), 0.0), axis=1, keepdims=True)
            COL[h, rows, :] = jnp.broadcast_to(weight, (cap, part))
            pick = jnp.where(hit, 1.0, 0.0).astype(bf)

            def tile(i, carry):
                lanes = pl.ds(pl.multiple_of(i * 256, 256), 256)
                XC[h, rows, lanes] = jnp.dot(pick, XT[slot, :, lanes], preferred_element_type=f32).astype(bf)
                return carry

            lax.fori_loop(0, width // 256, tile, 0)

    def spread(block, base, whose):
        eye = lax.broadcasted_iota(jnp.int32, (count, count), 0) == lax.broadcasted_iota(
            jnp.int32, (count, count), 1
        )
        for h in range(2):
            at = jnp.sum(jnp.where(eye, row_of(RK[block], whose[h]), 0.0), axis=1, keepdims=True)
            hit = lax.broadcasted_iota(jnp.int32, (count, cap), 1).astype(f32) == at
            EC[base + h] = jnp.where(hit, 1.0, 0.0).astype(bf)

    def hidden(low, high, a, b):
        h = low // 4
        rows = pl.ds(a * cap, (b - a) * cap)

        def one(s, carry):
            both = jnp.dot(XC[h, rows, :], GU[s], preferred_element_type=f32)
            gate, up = both[:, :part], both[:, part:]
            value = gate / (1.0 + jnp.exp(-gate)) * up * COL[h, rows, :]
            H[h, rows, pl.ds(pl.multiple_of((s - 4 * h) * part, part), part)] = value.astype(bf)
            return carry

        lax.fori_loop(low, high, one, 0)

    def times(left, right):
        return lax.dot_general(left, right, (((1,), (1,)), ((), ())), preferred_element_type=f32)

    def down(h, place, n, j):
        left = H[h, pl.ds(place * cap, n * cap), :]
        return times(left, DN[lane_block(j), pl.ds(h * 4 * part, 4 * part)]).astype(bf)

    def widen(block, base, halves):
        for h in halves:
            left = jnp.dot(EC[base + h], H[h, pl.ds(PLACE[block] * cap, cap), :], preferred_element_type=f32)
            HX[block, :, pl.ds(h * 4 * part, 4 * part)] = left.astype(bf)

    def total(block, base, at, j):
        rows = pl.ds(at * cap, cap)
        return (
            times(HX[block], DN[lane_block(j), :])
            + jnp.dot(EC[base], RN[j, rows, :], preferred_element_type=f32)
            + jnp.dot(EC[base + 1], RF[j, rows, :], preferred_element_type=f32)
        )

    for copy in own[:2]:
        copy.wait()
    own_routes()
    own[2].wait()
    pl.semaphore_wait(barrier, 5)
    for k in (1, 2):
        routes(k).start()
    for copy in own[3:5]:
        copy.wait()
    for j in range(CUTS):
        tokens(1, j).start()
        gu(4, j).start()
        if j == 0:
            tokens(2).start()
            gu(1).start()
        if j % (CUTS // NEAR_CUTS) == 0:
            gu(2, j * NEAR_CUTS // CUTS).start()
    own[5].wait()
    dn(1).start()
    dn(2).start()
    for j in range(AHEAD):
        dn(4, j).start()
    for copy in own[6:]:
        copy.wait()
    ranks(0)
    norm(0, 0, 0, count)
    gather(0, 0)
    spread(0, 0, mine)
    routes(1).wait_recv()
    routes(3).start()
    ranks(1)
    routes(2).wait_recv()
    ranks(2)
    spread(0, 2, of_x)

    def far(j):
        gu(4, j).wait_recv()
        gu(6, j).start()
        gu(5, j).start()

    def far_mate(j):
        gu(6, j).wait_recv()
        gu(7, j).start()

    def down_far(j):
        dn(4, j).wait_recv()
        if j + AHEAD < CUTS:
            dn(4, j + AHEAD).start()
        dn(6, j).start()
        dn(5, j).start()

    def down_mate(j):
        dn(6, j).wait_recv()
        dn(7, j).start()

    t_rows = count // CUTS
    for i in range(CUTS):
        tokens(1, i).wait_recv()
        tokens(3, i).start()
        far(i)
        if i < NEAR_CUTS:
            gu(2, i).wait_recv()
            gu(3, i).start()
        norm(1, 1, i * t_rows, (i + 1) * t_rows)
        if i == 0:
            spread(0, 4, of_z)
            spread(1, 6, mine)
        if i == 1:
            spread(1, 8, of_x)
            spread(2, 10, mine)
        if i == 2:
            spread(2, 12, of_z)
            routes(3).wait_recv()
            ranks(3)
        if i == NEAR_CUTS:
            tokens(2).wait_recv()
            norm(2, 0, 0, count)
            gather(2, 0)
            gu(1).wait_recv()
            gu(3).wait_recv()
            hidden(0, 4, 0, 2)
        if i == NEAR_CUTS + 1:
            dn(2).wait_recv()
            dn(3).start()
            far_mate(0)
        if i == NEAR_CUTS + 2:
            far_mate(1)
            dn(1).wait_recv()
            dn(3).wait_recv()
            for j in range(CUTS):
                if j not in Z_FIRST:
                    SN[j, :cap] = down(0, 1, 1, j)
                    first(0, j, pl.ds(0, cap)).start()
            far_mate(2)
    far_mate(3)
    gather(1, 1)
    tokens(3).wait_recv()
    norm(3, 0, 0, count)
    gather(3, 0)
    far_mate(4)
    hidden(0, 4, 2, 4)
    for j in range(CUTS):
        if j in Z_FIRST:
            SN[j] = down(0, 2, 2, j)
            first(1, j).start()
        else:
            SN[j, cap:] = down(0, 2, 1, j)
            first(1, j, pl.ds(cap, cap)).start()
    far_mate(5)
    down_far(0)
    widen(0, 0, (0,))
    widen(1, 6, (0,))
    widen(2, 10, (0,))
    gu(5).wait_recv()
    far_mate(6)
    hidden(4, 6, 0, 4)
    down_far(1)
    far_mate(7)
    down_far(2)
    gu(7).wait_recv()
    hidden(6, 8, 0, 4)
    down_mate(0)
    down_far(3)

    def pass_on(j):
        first(2, j).wait_recv()
        if j in Z_FIRST:
            first(1, j).wait_recv()
            kept, base, home, from_home, at = 2, 12, 4, 1, 0
        else:
            first(0, j, pl.ds(0, cap)).wait_recv()
            first(1, j, pl.ds(cap, cap)).wait_recv()
            kept, base, home, from_home, at = 1, 8, 2, 0, 1
        ZS[j] = total(kept, base, at, j).astype(bf)
        second(j).start()
        ACC[j] = total(0, home, from_home, j)

    for j in range(CUTS):
        if j + 4 < CUTS:
            down_far(j + 4)
        if j + 1 < CUTS:
            down_mate(j + 1)
        dn(5, j).wait_recv()
        dn(7, j).wait_recv()
        SF[j] = down(1, 2 if j in Z_FIRST else 1, 2, j)
        first(2, j).start()
        if j == 0:
            widen(0, 0, (1,))
            widen(1, 6, (1,))
            widen(2, 10, (1,))
        if j >= LAG:
            pass_on(j - LAG)
    for j in range(CUTS - LAG, CUTS):
        pass_on(j)
    square = jnp.zeros((count, 1), f32)
    for j in range(CUTS):
        second(j).wait_recv()
        mixed = ACC[j] + ZR[j].astype(f32)
        ACC[j] = mixed
        square = square + jnp.sum(mixed * mixed, axis=1, keepdims=True)
    scale = lax.rsqrt(square / width + 1e-06)
    for j in range(CUTS):
        out[:, lane_block(j)] = (ACC[j] * scale * POST[:, lane_block(j)]).astype(bf)
    for k in (1, 2, 3):
        routes(k).wait_send()
        tokens(k).wait_send()
    for k in range(1, 8):
        gu(k).wait_send()
        dn(k).wait_send()
    for kind, (src, dst) in enumerate(((SN, RN), (SF, RF), (ZS, ZR))):
        remote(src, dst, s_send.at[kind], z_recv.at[0], to_x).wait_send()


def fused(n_ep, tokens, pre_gain, post_gain, expert_ids, route_weight, w_gate, w_up, w_down):
    count, width = tokens.shape
    top = expert_ids.shape[1]
    part = w_gate.shape[2]
    experts = n_ep * w_gate.shape[0]
    cap = 2 * top * count // experts
    bf, f32 = jnp.bfloat16, jnp.float32
    cols = width // CUTS
    anywhere = pl.BlockSpec(memory_space=pl.ANY)
    vmem = pl.BlockSpec(memory_space=pltpu.VMEM)
    dma = pltpu.SemaphoreType.DMA
    return pl.pallas_call(
        functools.partial(kernel, n_ep),
        out_shape=jax.ShapeDtypeStruct((count, width), bf),
        in_specs=[anywhere] * 8,
        out_specs=vmem,
        scratch_shapes=[
            pltpu.VMEM((4, count, width), bf),
            pltpu.VMEM((2, count, width), bf),
            pltpu.VMEM((2, 4 * cap, width), bf),
            pltpu.VMEM((top, count), jnp.int32),
            pltpu.VMEM((top, count), f32),
            pltpu.VMEM((1, width), f32),
            pltpu.VMEM((1, width), f32),
            pltpu.VMEM((4, experts, count), f32),
            pltpu.VMEM((4, experts, count), f32),
            pltpu.VMEM((2, 4 * cap, part), f32),
            pltpu.VMEM((8, width, 2 * part), bf),
            pltpu.VMEM((width, 8 * part), bf),
            pltpu.VMEM((2, 4 * cap, 4 * part), bf),
            pltpu.VMEM((3, count, 8 * part), bf),
            pltpu.VMEM((14, count, cap), bf),
            pltpu.VMEM((CUTS, 2 * cap, cols), bf),
            pltpu.VMEM((CUTS, 2 * cap, cols), bf),
            pltpu.VMEM((CUTS, 2 * cap, cols), bf),
            pltpu.VMEM((CUTS, 2 * cap, cols), bf),
            pltpu.VMEM((CUTS, count, cols), bf),
            pltpu.VMEM((CUTS, count, cols), bf),
            pltpu.VMEM((CUTS, count, cols), f32),
            dma((8,)),
            dma((3,)), dma((CUTS,)), dma((3,)), dma((3,)), dma((3,)),
            dma((7,)), dma((7,)), dma((NEAR_CUTS,)), dma((2, CUTS)),
            dma((7,)), dma((3,)), dma((4, CUTS)),
            dma((3,)), dma((CUTS,)), dma((CUTS,)), dma((CUTS,)), dma((CUTS,)),
        ],
        compiler_params=pltpu.CompilerParams(
            collective_id=0, has_side_effects=True, vmem_limit_bytes=VMEM_BYTES
        ),
    )(tokens, pre_gain[None], post_gain[None], expert_ids.T, route_weight.T, w_gate, w_up, w_down)


def whole_body(n_ep, n_tp, *args):
    lanes = args[5].shape[2]
    if n_ep // 2 == n_tp == 2 * 2 and args[5].shape[0] == 1 and lanes % 128 == 0:
        return fused(n_ep, *args)
    return body(*args)


def solution(mesh):
    in_specs = (
        P(("ep", "tp"), None),
        P(),
        P(),
        P(("ep", "tp"), None),
        P(("ep", "tp"), None),
        P("ep", None, "tp"),
        P("ep", None, "tp"),
        P("ep", None, "tp"),
    )
    out_specs = P(("ep", "tp"), None)
    step = functools.partial(whole_body, mesh.shape["ep"], mesh.shape["tp"])
    return jax.shard_map(step, mesh=mesh, in_specs=in_specs, out_specs=out_specs, check_vma=False)
```

time: 121 us -> 111 us (0.917); the launches traced: 119 us -> 111 us
  Pallas kernels: 116 us -> 108 us
    pallas_call x1, Pallas kernels: 116 us -> 108 us  [fused(): pl.pallas_call(functools.partial(kernel, n_ep), out_shape=jax.ShapeDtypeS...]
    unnamed x5 -> x1, local copies, waits for them, and re-layouts: 3 us -> 2.3 us
where the time goes in v1:
time: 111 us
  Pallas kernels  108 us (97%)
  local copies, waits for them, and re-layouts  2.3 us (2%)
    pallas_call x1, Pallas kernels, fused(): pl.pallas_call(functools.partial(kernel, n_ep), out_shape=jax.ShapeDtypeS...  108 us
    unnamed x1, local copies, waits for them, and re-layouts  2.3 us

profile of v1, /device:TPU:0, one launch (start us, length us, event | category | flops | bytes accessed | tf_op | source)
XLA Modules:
  0.0 110.7 jit_solution(5277159752814887943)
XLA Ops:
  0.0 108.4 %shard_map.82 = bf16[256,2048]{1,0:T(8,128)(2,1)} custom-call(bf16[256,2048]{1,0:T(8,128)(2,1)} %tok.1, f32[1,2048]{1,0:T(1,128)} %bitcast.4, f32[1,2048]{1,0:T(1,128)} %bitcast.5, s32[2,256]{1,0:T(2,128)} %bitcast.6, f32[2,256]{1,0:T(2,128)} %bitcast.7, bf16[1,2048,128]{2,1,0:T(8,128)(2,1)} %wg.1, bf16[1,2048,128]{2,1,0:T(8,128)(2,1)} %wu.1, ...), custom_call_target="tpu_custom_call" | custom-call | tf_op jit(solution)/shard_map/pallas_call | solution.py:438
  108.4 2.3 %copy.10 = bf16[256,2048]{1,0:T(8,128)(2,1)} copy(bf16[256,2048]{1,0:T(8,128)(2,1)} %shard_map.82) | data formatting | bytes 2097152

commit v2 on v1

--- a/solution.py
+++ b/solution.py
@@ -59,7 +59,7 @@
 NEAR_CUTS = 4
 LAG = 3
 AHEAD = 4
-Z_FIRST = (0, 4)
+Z_FIRST = (2, 5)
 PLACE = (0, 3, 1, 2)
 VMEM_BYTES = 60 * 2**20
 
@@ -70,7 +70,7 @@
 
 def kernel(
     n_ep, tok, pre, post, ids, rw, wg, wu, wd, out,
-    T, XT, XC, IDS, RW, PRE, POST, WR, RK, COL, GU, DN, H, HX, EC, SN, SF, RN, RF, ZS, ZR, ACC,
+    T, X, XC, IDS, RW, PRE, POST, WR, RK, COL, GU, DN, H, HX, EC, SN, SF, RN, RF, ZS, ZR, ACC,
     loc, t_send, t1_recv, t_recv, w_send, w_recv, g_send, g_recv, g2_recv, gf_recv, d_send, d_recv, df_recv,
     s_send, n_recv, m_recv, f_recv, z_recv,
 ):
@@ -91,7 +91,7 @@
     own = [
         pltpu.make_async_copy(ids, IDS, loc.at[0]),
         pltpu.make_async_copy(rw, RW, loc.at[1]),
-        pltpu.make_async_copy(tok, T.at[0], loc.at[2]),
+        pltpu.make_async_copy(tok, T, loc.at[2]),
         pltpu.make_async_copy(wg.at[0], GU.at[0, :, pl.ds(0, part)], loc.at[3]),
         pltpu.make_async_copy(wu.at[0], GU.at[0, :, pl.ds(part, part)], loc.at[4]),
         pltpu.make_async_copy(wd.at[0], DN.at[:, pl.ds(0, part)], loc.at[5]),
@@ -119,7 +119,7 @@
         s, who = block_from[k]
         rows = rows_of(count, CUTS, j)
         recv = t1_recv.at[j] if k == 1 and j is not None else t_recv.at[k - 1]
-        return remote(T.at[s, rows], T.at[k, rows], t_send.at[k - 1], recv, who)
+        return remote(X.at[s, rows], X.at[k, rows], t_send.at[k - 1], recv, who)
 
     def route(k):
         if k % 2:
@@ -184,30 +184,30 @@
         upto = jnp.dot(ones, jnp.where(before, 1.0, 0.0), preferred_element_type=f32)
         RK[block] = jnp.where(named, upto - 1.0, -1.0)
 
-    def norm(block, slot, low, high):
+    def norm():
         def some(i, carry):
             rows = pl.ds(pl.multiple_of(i * 16, 16), 16)
-            values = T[block, rows, :].astype(f32)
-            XT[slot, rows, :] = rms_scale(values, PRE[...]).astype(bf)
+            X[0, rows, :] = rms_scale(T[rows, :].astype(f32), PRE[...]).astype(bf)
             return carry
 
-        lax.fori_loop(low // 16, high // 16, some, 0)
-
-    def gather(block, slot):
+        lax.fori_loop(0, count // 16, some, 0, unroll=4)
+
+    def gather(block):
         rows = pl.ds(PLACE[block] * cap, cap)
+        picks = []
         for h in range(2):
             at = row_of(RK[block], mine[h])
             hit = lax.broadcasted_iota(jnp.int32, (cap, count), 0).astype(f32) == at
             weight = jnp.sum(jnp.where(hit, row_of(WR[block], mine[h]), 0.0), axis=1, keepdims=True)
             COL[h, rows, :] = jnp.broadcast_to(weight, (cap, part))
-            pick = jnp.where(hit, 1.0, 0.0).astype(bf)
-
-            def tile(i, carry):
-                lanes = pl.ds(pl.multiple_of(i * 256, 256), 256)
-                XC[h, rows, lanes] = jnp.dot(pick, XT[slot, :, lanes], preferred_element_type=f32).astype(bf)
-                return carry
-
-            lax.fori_loop(0, width // 256, tile, 0)
+            picks.append(jnp.where(hit, 1.0, 0.0).astype(bf))
+        pick = jnp.concatenate(picks, axis=0)
+        step = width // 4
+        for i in range(4):
+            lanes = pl.ds(i * step, step)
+            found = jnp.dot(pick, X[block, :, lanes], preferred_element_type=f32).astype(bf)
+            XC[0, rows, lanes] = found[:cap]
+            XC[1, rows, lanes] = found[cap:]
 
     def spread(block, base, whose):
         eye = lax.broadcasted_iota(jnp.int32, (count, count), 0) == lax.broadcasted_iota(
@@ -255,6 +255,8 @@
         copy.wait()
     own_routes()
     own[2].wait()
+    own[6].wait()
+    norm()
     pl.semaphore_wait(barrier, 5)
     for k in (1, 2):
         routes(k).start()
@@ -273,16 +275,14 @@
     dn(2).start()
     for j in range(AHEAD):
         dn(4, j).start()
-    for copy in own[6:]:
-        copy.wait()
+    own[7].wait()
     ranks(0)
-    norm(0, 0, 0, count)
-    gather(0, 0)
-    spread(0, 0, mine)
     routes(1).wait_recv()
     routes(3).start()
+    routes(2).wait_recv()
+    gather(0)
+    spread(0, 0, mine)
     ranks(1)
-    routes(2).wait_recv()
     ranks(2)
     spread(0, 2, of_x)
 
@@ -306,7 +306,11 @@
         dn(6, j).wait_recv()
         dn(7, j).start()
 
-    t_rows = count // CUTS
+    def near(j):
+        SN[j, :cap] = down(0, 1, 1, j)
+        first(0, j, pl.ds(0, cap)).start()
+
+    x_first = [j for j in range(CUTS) if j not in Z_FIRST]
     for i in range(CUTS):
         tokens(1, i).wait_recv()
         tokens(3, i).start()
@@ -314,7 +318,6 @@
         if i < NEAR_CUTS:
             gu(2, i).wait_recv()
             gu(3, i).start()
-        norm(1, 1, i * t_rows, (i + 1) * t_rows)
         if i == 0:
             spread(0, 4, of_z)
             spread(1, 6, mine)
@@ -323,12 +326,12 @@
             spread(2, 10, mine)
         if i == 2:
             spread(2, 12, of_z)
+        if i == NEAR_CUTS - 1:
             routes(3).wait_recv()
             ranks(3)
         if i == NEAR_CUTS:
             tokens(2).wait_recv()
-            norm(2, 0, 0, count)
-            gather(2, 0)
+            gather(2)
             gu(1).wait_recv()
             gu(3).wait_recv()
             hidden(0, 4, 0, 2)
@@ -336,43 +339,39 @@
             dn(2).wait_recv()
             dn(3).start()
             far_mate(0)
+            dn(1).wait_recv()
+            dn(3).wait_recv()
+            near(x_first[0])
         if i == NEAR_CUTS + 2:
             far_mate(1)
-            dn(1).wait_recv()
-            dn(3).wait_recv()
-            for j in range(CUTS):
-                if j not in Z_FIRST:
-                    SN[j, :cap] = down(0, 1, 1, j)
-                    first(0, j, pl.ds(0, cap)).start()
+            near(x_first[1])
             far_mate(2)
+    gather(1)
+    for j in x_first[2:]:
+        near(j)
     far_mate(3)
-    gather(1, 1)
     tokens(3).wait_recv()
-    norm(3, 0, 0, count)
-    gather(3, 0)
+    gather(3)
     far_mate(4)
     hidden(0, 4, 2, 4)
-    for j in range(CUTS):
-        if j in Z_FIRST:
-            SN[j] = down(0, 2, 2, j)
-            first(1, j).start()
-        else:
-            SN[j, cap:] = down(0, 2, 1, j)
-            first(1, j, pl.ds(cap, cap)).start()
+    for j in x_first:
+        SN[j, cap:] = down(0, 2, 1, j)
+        first(1, j, pl.ds(cap, cap)).start()
     far_mate(5)
+    for j in Z_FIRST:
+        SN[j] = down(0, 2, 2, j)
+        first(1, j).start()
     down_far(0)
+    far_mate(6)
+    gu(5).wait_recv()
+    hidden(4, 6, 0, 4)
+    far_mate(7)
+    down_far(1)
+    down_far(2)
     widen(0, 0, (0,))
-    widen(1, 6, (0,))
-    widen(2, 10, (0,))
-    gu(5).wait_recv()
-    far_mate(6)
-    hidden(4, 6, 0, 4)
-    down_far(1)
-    far_mate(7)
-    down_far(2)
+    down_mate(0)
     gu(7).wait_recv()
     hidden(6, 8, 0, 4)
-    down_mate(0)
     down_far(3)
 
     def pass_on(j):
@@ -389,18 +388,18 @@
         ACC[j] = total(0, home, from_home, j)
 
     for j in range(CUTS):
-        if j + 4 < CUTS:
-            down_far(j + 4)
         if j + 1 < CUTS:
             down_mate(j + 1)
         dn(5, j).wait_recv()
         dn(7, j).wait_recv()
         SF[j] = down(1, 2 if j in Z_FIRST else 1, 2, j)
         first(2, j).start()
+        if j + 4 < CUTS:
+            down_far(j + 4)
         if j == 0:
+            widen(1, 6, (0, 1))
+            widen(2, 10, (0, 1))
             widen(0, 0, (1,))
-            widen(1, 6, (1,))
-            widen(2, 10, (1,))
         if j >= LAG:
             pass_on(j - LAG)
     for j in range(CUTS - LAG, CUTS):
@@ -441,8 +440,8 @@
         in_specs=[anywhere] * 8,
         out_specs=vmem,
         scratch_shapes=[
+            pltpu.VMEM((count, width), bf),
             pltpu.VMEM((4, count, width), bf),
-            pltpu.VMEM((2, count, width), bf),
             pltpu.VMEM((2, 4 * cap, width), bf),
             pltpu.VMEM((top, count), jnp.int32),
             pltpu.VMEM((top, count), f32),

time: 111 us -> 103 us (0.928)
  Pallas kernels: 108 us -> 101 us
    pallas_call x1, Pallas kernels: 108 us -> 101 us  [fused(): pl.pallas_call(functools.partial(kernel, n_ep), out_shape=jax.ShapeDtypeS...]
where the time goes in v2:
time: 103 us
  Pallas kernels  101 us (98%)
  local copies, waits for them, and re-layouts  2.3 us (2%)
    pallas_call x1, Pallas kernels, fused(): pl.pallas_call(functools.partial(kernel, n_ep), out_shape=jax.ShapeDtypeS...  101 us
    unnamed x1, local copies, waits for them, and re-layouts  2.3 us

profile of v2, /device:TPU:0, one launch (start us, length us, event | category | flops | bytes accessed | tf_op | source)
XLA Modules:
  0.0 103.0 jit_solution(9569445931322614746)
XLA Ops:
  0.0 100.7 %shard_map.82 = bf16[256,2048]{1,0:T(8,128)(2,1)} custom-call(bf16[256,2048]{1,0:T(8,128)(2,1)} %tok.1, f32[1,2048]{1,0:T(1,128)} %bitcast.4, f32[1,2048]{1,0:T(1,128)} %bitcast.5, s32[2,256]{1,0:T(2,128)} %bitcast.6, f32[2,256]{1,0:T(2,128)} %bitcast.7, bf16[1,2048,128]{2,1,0:T(8,128)(2,1)} %wg.1, bf16[1,2048,128]{2,1,0:T(8,128)(2,1)} %wu.1, ...), custom_call_target="tpu_custom_call" | custom-call | tf_op jit(solution)/shard_map/pallas_call | solution.py:437
  100.7 2.3 %copy.10 = bf16[256,2048]{1,0:T(8,128)(2,1)} copy(bf16[256,2048]{1,0:T(8,128)(2,1)} %shard_map.82) | data formatting | bytes 2097152

commit v3 on v2

--- a/solution.py
+++ b/solution.py
@@ -57,9 +57,8 @@
 MESH = pl.DeviceIdType.MESH
 CUTS = 8
 NEAR_CUTS = 4
-LAG = 3
 AHEAD = 4
-Z_FIRST = (2, 5)
+Z_FIRST = (0,)
 PLACE = (0, 3, 1, 2)
 VMEM_BYTES = 60 * 2**20
 
@@ -72,7 +71,7 @@
     n_ep, tok, pre, post, ids, rw, wg, wu, wd, out,
     T, X, XC, IDS, RW, PRE, POST, WR, RK, COL, GU, DN, H, HX, EC, SN, SF, RN, RF, ZS, ZR, ACC,
     loc, t_send, t1_recv, t_recv, w_send, w_recv, g_send, g_recv, g2_recv, gf_recv, d_send, d_recv, df_recv,
-    s_send, n_recv, m_recv, f_recv, z_recv,
+    s_send, n_recv, m_recv, f_recv, h_recv, z_recv,
 ):
     count, width = tok.shape
     part = wg.shape[2]
@@ -154,7 +153,7 @@
     def first(kind, j, rows=None):
         src, dst = (SN, RN) if kind < 2 else (SF, RF)
         rows = pl.ds(0, 2 * cap) if rows is None else rows
-        recv = (n_recv, m_recv, f_recv)[kind].at[j]
+        recv = (n_recv, m_recv, f_recv, h_recv)[kind].at[j]
         return remote(src.at[j, rows], dst.at[j, rows], s_send.at[kind // 2], recv, to_z if j in Z_FIRST else to_x)
 
     def second(j):
@@ -310,102 +309,212 @@
         SN[j, :cap] = down(0, 1, 1, j)
         first(0, j, pl.ds(0, cap)).start()
 
+    def chunk(j):
+        if j in Z_FIRST:
+            return 2, 12, 4, 1, 0
+        return 1, 8, 2, 0, 1
+
+    def parts(j):
+        near_rows, far_rows = pl.ds(0, cap), pl.ds(cap, cap)
+        return (far_rows, near_rows) if j in Z_FIRST else (near_rows, far_rows)
+
+    def relay(j):
+        kept, base, _, _, at = chunk(j)
+        first(2, j, parts(j)[1]).wait_recv()
+        if j in Z_FIRST:
+            first(1, j).wait_recv()
+        else:
+            first(0, j, pl.ds(0, cap)).wait_recv()
+            first(1, j, pl.ds(cap, cap)).wait_recv()
+        ZS[j] = total(kept, base, at, j).astype(bf)
+        second(j).start()
+
+    def settle(j):
+        _, _, base, at, _ = chunk(j)
+        first(3, j, parts(j)[0]).wait_recv()
+        ACC[j] = total(0, base, at, j)
+
     x_first = [j for j in range(CUTS) if j not in Z_FIRST]
-    for i in range(CUTS):
+
+    def near(i):
+        if i < len(x_first):
+            SN[x_first[i], :cap] = down(0, 1, 1, x_first[i])
+            first(0, x_first[i], pl.ds(0, cap)).start()
+
+    def diagonal(j):
+        if j in Z_FIRST:
+            SN[j] = down(0, 2, 2, j)
+            first(1, j).start()
+        else:
+            SN[j, cap:] = down(0, 2, 1, j)
+            first(1, j, pl.ds(cap, cap)).start()
+
+    def foreign(j):
+        dn(5, j).wait_recv()
+        dn(7, j).wait_recv()
+        SF[j] = down(1, 2 if j in Z_FIRST else 1, 2, j)
+        first(2, j, parts(j)[1]).start()
+
+    def push(j):
+        first(3, j, parts(j)[0]).start()
+
+    def one_token(i):
         tokens(1, i).wait_recv()
         tokens(3, i).start()
-        far(i)
-        if i < NEAR_CUTS:
-            gu(2, i).wait_recv()
-            gu(3, i).start()
-        if i == 0:
-            spread(0, 4, of_z)
-            spread(1, 6, mine)
-        if i == 1:
-            spread(1, 8, of_x)
-            spread(2, 10, mine)
-        if i == 2:
-            spread(2, 12, of_z)
-        if i == NEAR_CUTS - 1:
-            routes(3).wait_recv()
-            ranks(3)
-        if i == NEAR_CUTS:
-            tokens(2).wait_recv()
-            gather(2)
-            gu(1).wait_recv()
-            gu(3).wait_recv()
-            hidden(0, 4, 0, 2)
-        if i == NEAR_CUTS + 1:
-            dn(2).wait_recv()
-            dn(3).start()
-            far_mate(0)
-            dn(1).wait_recv()
-            dn(3).wait_recv()
-            near(x_first[0])
-        if i == NEAR_CUTS + 2:
-            far_mate(1)
-            near(x_first[1])
-            far_mate(2)
+
+    def near_mate(i):
+        gu(2, i).wait_recv()
+        gu(3, i).start()
+
+    def block_two():
+        tokens(2).wait_recv()
+        gather(2)
+
+    def native_early():
+        gu(1).wait_recv()
+        gu(3).wait_recv()
+        hidden(0, 4, 0, 2)
+
+    def down_two():
+        dn(2).wait_recv()
+        dn(3).start()
+
+    def down_near():
+        dn(1).wait_recv()
+        dn(3).wait_recv()
+
+    def block_three():
+        tokens(3).wait_recv()
+        gather(3)
+
+    def far_low():
+        gu(5).wait_recv()
+        hidden(4, 6, 0, 4)
+
+    def far_high():
+        gu(7).wait_recv()
+        hidden(6, 8, 0, 4)
+
+    def routes_three():
+        routes(3).wait_recv()
+        ranks(3)
+
+    def widen_all(h):
+        widen(1, 6, (h,))
+        widen(2, 10, (h,))
+        widen(0, 0, (h,))
+
+    one_token(0)
+    far(0)
+    near_mate(0)
+    spread(0, 4, of_z)
+    spread(1, 6, mine)
+    one_token(1)
+    far(1)
+    near_mate(1)
+    spread(1, 8, of_x)
+    spread(2, 10, mine)
+    one_token(2)
+    far(2)
+    near_mate(2)
+    spread(2, 12, of_z)
+    one_token(3)
+    far(3)
+    near_mate(3)
+    routes_three()
+    one_token(4)
+    far(4)
+    block_two()
+    native_early()
+    one_token(5)
+    far(5)
+    down_two()
+    far_mate(0)
+    down_near()
+    near(0)
+    one_token(6)
+    far(6)
+    far_mate(1)
+    near(1)
+    far_mate(2)
+    one_token(7)
+    far(7)
     gather(1)
-    for j in x_first[2:]:
-        near(j)
+    near(2)
+    near(3)
+    near(4)
+    near(5)
+    near(6)
+    near(7)
     far_mate(3)
-    tokens(3).wait_recv()
-    gather(3)
+    block_three()
     far_mate(4)
     hidden(0, 4, 2, 4)
-    for j in x_first:
-        SN[j, cap:] = down(0, 2, 1, j)
-        first(1, j, pl.ds(cap, cap)).start()
+    diagonal(1)
+    diagonal(2)
+    diagonal(3)
+    diagonal(4)
+    diagonal(5)
+    diagonal(6)
+    diagonal(7)
     far_mate(5)
-    for j in Z_FIRST:
-        SN[j] = down(0, 2, 2, j)
-        first(1, j).start()
+    diagonal(0)
     down_far(0)
     far_mate(6)
-    gu(5).wait_recv()
-    hidden(4, 6, 0, 4)
+    far_low()
     far_mate(7)
     down_far(1)
     down_far(2)
-    widen(0, 0, (0,))
+    widen_all(0)
     down_mate(0)
-    gu(7).wait_recv()
-    hidden(6, 8, 0, 4)
+    far_high()
     down_far(3)
-
-    def pass_on(j):
-        first(2, j).wait_recv()
-        if j in Z_FIRST:
-            first(1, j).wait_recv()
-            kept, base, home, from_home, at = 2, 12, 4, 1, 0
-        else:
-            first(0, j, pl.ds(0, cap)).wait_recv()
-            first(1, j, pl.ds(cap, cap)).wait_recv()
-            kept, base, home, from_home, at = 1, 8, 2, 0, 1
-        ZS[j] = total(kept, base, at, j).astype(bf)
-        second(j).start()
-        ACC[j] = total(0, home, from_home, j)
-
-    for j in range(CUTS):
-        if j + 1 < CUTS:
-            down_mate(j + 1)
-        dn(5, j).wait_recv()
-        dn(7, j).wait_recv()
-        SF[j] = down(1, 2 if j in Z_FIRST else 1, 2, j)
-        first(2, j).start()
-        if j + 4 < CUTS:
-            down_far(j + 4)
-        if j == 0:
-            widen(1, 6, (0, 1))
-            widen(2, 10, (0, 1))
-            widen(0, 0, (1,))
-        if j >= LAG:
-            pass_on(j - LAG)
-    for j in range(CUTS - LAG, CUTS):
-        pass_on(j)
+    down_mate(1)
+    foreign(0)
+    down_mate(2)
+    foreign(1)
+    widen_all(1)
+    down_far(4)
+    down_mate(3)
+    foreign(2)
+    down_far(5)
+    push(0)
+    down_mate(4)
+    foreign(3)
+    down_far(6)
+    push(1)
+    relay(1)
+    down_mate(5)
+    foreign(4)
+    down_far(7)
+    push(2)
+    relay(2)
+    down_mate(6)
+    foreign(5)
+    push(3)
+    relay(3)
+    down_mate(7)
+    foreign(6)
+    push(4)
+    relay(4)
+    foreign(7)
+    push(5)
+    relay(5)
+    push(6)
+    push(7)
+    relay(0)
+    settle(0)
+    settle(1)
+    relay(6)
+    settle(2)
+    settle(3)
+    relay(7)
+    settle(4)
+    settle(5)
+    settle(6)
+    settle(7)
     square = jnp.zeros((count, 1), f32)
-    for j in range(CUTS):
+    for j in (1, 2, 3, 4, 5, 0, 6, 7):
         second(j).wait_recv()
         mixed = ACC[j] + ZR[j].astype(f32)
         ACC[j] = mixed
@@ -466,7 +575,7 @@
             dma((3,)), dma((CUTS,)), dma((3,)), dma((3,)), dma((3,)),
             dma((7,)), dma((7,)), dma((NEAR_CUTS,)), dma((2, CUTS)),
             dma((7,)), dma((3,)), dma((4, CUTS)),
-            dma((3,)), dma((CUTS,)), dma((CUTS,)), dma((CUTS,)), dma((CUTS,)),
+            dma((3,)), dma((CUTS,)), dma((CUTS,)), dma((CUTS,)), dma((CUTS,)), dma((CUTS,)),
         ],
         compiler_params=pltpu.CompilerParams(
             collective_id=0, has_side_effects=True, vmem_limit_bytes=VMEM_BYTES

time: 103 us -> 101 us (0.981)
  Pallas kernels: 101 us -> 98.6 us
    pallas_call x1, Pallas kernels: 101 us -> 98.6 us  [fused(): pl.pallas_call(functools.partial(kernel, n_ep), out_shape=jax.ShapeDtypeS...]
where the time goes in v3:
time: 101 us
  Pallas kernels  98.6 us (98%)
  local copies, waits for them, and re-layouts  2.3 us (2%)
    pallas_call x1, Pallas kernels, fused(): pl.pallas_call(functools.partial(kernel, n_ep), out_shape=jax.ShapeDtypeS...  98.6 us
    unnamed x1, local copies, waits for them, and re-layouts  2.3 us

profile of v3, /device:TPU:0, one launch (start us, length us, event | category | flops | bytes accessed | tf_op | source)
XLA Modules:
  0.0 100.9 jit_solution(9255613158263372585)
XLA Ops:
  0.0 98.6 %shard_map.82 = bf16[256,2048]{1,0:T(8,128)(2,1)} custom-call(bf16[256,2048]{1,0:T(8,128)(2,1)} %tok.1, f32[1,2048]{1,0:T(1,128)} %bitcast.4, f32[1,2048]{1,0:T(1,128)} %bitcast.5, s32[2,256]{1,0:T(2,128)} %bitcast.6, f32[2,256]{1,0:T(2,128)} %bitcast.7, bf16[1,2048,128]{2,1,0:T(8,128)(2,1)} %wg.1, bf16[1,2048,128]{2,1,0:T(8,128)(2,1)} %wu.1, ...), custom_call_target="tpu_custom_call" | custom-call | tf_op jit(solution)/shard_map/pallas_call | solution.py:546
  98.6 2.3 %copy.10 = bf16[256,2048]{1,0:T(8,128)(2,1)} copy(bf16[256,2048]{1,0:T(8,128)(2,1)} %shard_map.82) | data formatting | bytes 2097152

commit v4 on v3

--- a/solution.py
+++ b/solution.py
@@ -391,9 +391,12 @@
         gu(5).wait_recv()
         hidden(4, 6, 0, 4)
 
+    def far_mid():
+        hidden(6, 7, 0, 4)
+
     def far_high():
         gu(7).wait_recv()
-        hidden(6, 8, 0, 4)
+        hidden(7, 8, 0, 4)
 
     def routes_three():
         routes(3).wait_recv()
@@ -458,14 +461,15 @@
     diagonal(6)
     diagonal(7)
     far_mate(5)
-    diagonal(0)
     down_far(0)
     far_mate(6)
+    diagonal(0)
     far_low()
     far_mate(7)
     down_far(1)
     down_far(2)
     widen_all(0)
+    far_mid()
     down_mate(0)
     far_high()
     down_far(3)
@@ -478,28 +482,28 @@
     down_mate(3)
     foreign(2)
     down_far(5)
-    push(0)
     down_mate(4)
     foreign(3)
     down_far(6)
-    push(1)
+    push(0)
     relay(1)
     down_mate(5)
     foreign(4)
     down_far(7)
-    push(2)
+    push(1)
     relay(2)
     down_mate(6)
     foreign(5)
-    push(3)
+    push(2)
     relay(3)
     down_mate(7)
     foreign(6)
-    push(4)
+    push(3)
     relay(4)
     foreign(7)
+    push(4)
+    relay(5)
     push(5)
-    relay(5)
     push(6)
     push(7)
     relay(0)

time: 101 us -> 101 us (level)
  no operation moved by 1% of the time
where the time goes in v4:
time: 101 us
  Pallas kernels  98.7 us (98%)
  local copies, waits for them, and re-layouts  2.3 us (2%)
    pallas_call x1, Pallas kernels, fused(): pl.pallas_call(functools.partial(kernel, n_ep), out_shape=jax.ShapeDtypeS...  98.7 us
    unnamed x1, local copies, waits for them, and re-layouts  2.3 us

profile of v4, /device:TPU:0, one launch (start us, length us, event | category | flops | bytes accessed | tf_op | source)
XLA Modules:
  0.0 101.0 jit_solution(1371754734585776741)
XLA Ops:
  0.0 98.7 %shard_map.82 = bf16[256,2048]{1,0:T(8,128)(2,1)} custom-call(bf16[256,2048]{1,0:T(8,128)(2,1)} %tok.1, f32[1,2048]{1,0:T(1,128)} %bitcast.4, f32[1,2048]{1,0:T(1,128)} %bitcast.5, s32[2,256]{1,0:T(2,128)} %bitcast.6, f32[2,256]{1,0:T(2,128)} %bitcast.7, bf16[1,2048,128]{2,1,0:T(8,128)(2,1)} %wg.1, bf16[1,2048,128]{2,1,0:T(8,128)(2,1)} %wu.1, ...), custom_call_target="tpu_custom_call" | custom-call | tf_op jit(solution)/shard_map/pallas_call | solution.py:550
  98.7 2.3 %copy.10 = bf16[256,2048]{1,0:T(8,128)(2,1)} copy(bf16[256,2048]{1,0:T(8,128)(2,1)} %shard_map.82) | data formatting | bytes 2097152
